TPU v7x, 128 devices: a whole 4x4x4 slice. The times are simulated.
128 devices in a mesh: ep: 16 (over z, x), tp: 8 (over y, core).
Axes of the slice: x: 4, y: 4, z: 4, core: 2. Of those that a mesh axis runs over, the one named last changes fastest.
Arguments:
- mix_tokens: bfloat16 [32768, 2048], P(('ep', 'tp')), may hold values from -40 to 40
- mix_gain: float32 [2048], replicated, may hold values from 0.1 to 1.9
- query_weight: bfloat16 [2048, 1024], replicated, may hold values from -0.125 to 0.125
- key_weight: bfloat16 [2048, 256], replicated, may hold values from -0.125 to 0.125
- value_weight: bfloat16 [2048, 256], replicated, may hold values from -0.125 to 0.125
- query_gain: float32 [64], replicated, may hold values from 0.5 to 40
- key_gain: float32 [64], replicated, may hold values from 0.1 to 1.9
- sink_logits: float32 [16], replicated, may hold values from 2 to 6
- out_weight: bfloat16 [1024, 2048], replicated, may hold values from -0.1875 to 0.1875
- moe_tokens: bfloat16 [16384, 2048], P(('ep', 'tp')), may hold values from -40 to 40
- moe_gain: float32 [2048], replicated, may hold values from 0.1 to 1.9
- routes: int32 [16384, 2], P(('ep', 'tp')), may hold values from 0 to 15, all different within a row; in each aligned block of 128 rows (0 to 127, 128 to 255, ...) at most 18 rows name the same one
- route_logits: float32 [16384, 2], P(('ep', 'tp')), may hold values from -6 to 6
- gate_weight: bfloat16 [16, 2048, 7168], P('ep', None, 'tp'), may hold values from -0.125 to 0.125
- up_weight: bfloat16 [16, 2048, 7168], P('ep', None, 'tp'), may hold values from -0.125 to 0.125
- down_weight: bfloat16 [16, 7168, 2048], P('ep', 'tp'), may hold values from -0.0625 to 0.0625
Outputs:
- mix_out: bfloat16 [32768, 2048], P(('ep', 'tp'))
- moe_out: bfloat16 [16384, 2048], P(('ep', 'tp'))
Inputs may be any that keep to these rules, and one draw needn't show every extreme that they name: `routes`: each row names 2 different experts. Of the rows of one device no expert is named more than 18 times, and in every draw some device names some expert exactly 18 times.
All inputs are finite; a program needn't handle non-finite values.
Results may differ from a plain program's by a relative error of at most 0.015.
The roundings to bfloat16 on the way count: a program that leaves them out, or rounds other values in their place, can miss the bound.
Values may be sent and summed in bfloat16 or wider, within the bound.
No kernel may reach another device: no remote copies, remote signals or barrier semaphores. Data moves between devices by JAX's collectives and lax.ppermute only.
A program may use at most 128 MiB of HBM per device.

v0:
```python
import jax
import jax.numpy as jnp
from jax import lax
from jax.sharding import PartitionSpec as P

WINDOW = 128
epsilon = 1e-06


def passed_along(block, axis, distance):
    devices = range(lax.axis_size(axis))
    route = [(i - distance, i) for i in devices if i - distance in devices]
    return lax.ppermute(block, axis, route)


def rms_scale(values, gain_vec):
    values = values.astype(jnp.float32)
    return (
        values * lax.rsqrt(jnp.mean(values * values, axis=-1, keepdims=True) + epsilon) * gain_vec
    )


def route_slots(routes, experts, capacity):
    flat_ids = routes.reshape(-1)
    onehot = (flat_ids[:, None] == jnp.arange(experts, dtype=jnp.int32)[None, :]).astype(jnp.int32)
    before = jnp.cumsum(onehot, axis=0) - onehot
    slot_ids = jnp.sum(before * onehot, axis=1)
    return (flat_ids * capacity + slot_ids).reshape(routes.shape)


def window_attention(queries, key_ext, value_ext, sink_logits, first_pos):
    row_count = queries.shape[0]
    window_rows = key_ext.shape[0] - row_count
    blocks = row_count // window_rows
    kv_heads = key_ext.shape[1]
    group_size = queries.shape[1] // kv_heads
    head_dim = queries.shape[2]
    query_blk = queries.reshape(blocks, window_rows, kv_heads, group_size, head_dim)

    def pair_up(source):
        lower = source[:row_count].reshape(blocks, window_rows, kv_heads, head_dim)
        upper = source[window_rows:].reshape(blocks, window_rows, kv_heads, head_dim)
        return jnp.concatenate([lower, upper], axis=1)

    key_blk = pair_up(key_ext)
    value_blk = pair_up(value_ext)
    scores = jnp.einsum(
        "bqkgd,bskd->bkgqs", query_blk, key_blk, preferred_element_type=jnp.float32
    ) * head_dim ** (-0.5)
    query_pos = jnp.arange(window_rows, dtype=jnp.int32)[:, None] + window_rows
    key_pos = jnp.arange(2 * window_rows, dtype=jnp.int32)[None, :]
    pos_gap = query_pos - key_pos
    block_start = first_pos + jnp.arange(blocks, dtype=jnp.int32) * window_rows - window_rows
    key_global = block_start[:, None] + jnp.arange(2 * window_rows, dtype=jnp.int32)[None, :]
    visible = ((pos_gap >= 0) & (pos_gap <= window_rows))[None] & (key_global >= 0)[:, None, :]
    scores = jnp.where(visible[:, None, None], scores, -jnp.inf)
    sink_col = sink_logits.reshape(kv_heads, group_size)[None, :, :, None, None]
    row_top = jnp.maximum(jnp.max(scores, axis=-1, keepdims=True), sink_col)
    weights = jnp.exp(scores - row_top)
    denom_sum = jnp.sum(weights, axis=-1, keepdims=True) + jnp.exp(sink_col - row_top)
    attn_prob = (weights / denom_sum).astype(jnp.bfloat16)
    mixed_out = jnp.einsum(
        "bkgqs,bskd->bqkgd", attn_prob, value_blk, preferred_element_type=jnp.float32
    )
    return mixed_out.astype(jnp.bfloat16).reshape(row_count, -1)


def body(
    mix_tokens,
    mix_gain,
    query_weight,
    key_weight,
    value_weight,
    query_gain,
    key_gain,
    sink_logits,
    out_weight,
    moe_tokens,
    moe_gain,
    routes,
    route_logits,
    gate_weight,
    up_weight,
    down_weight,
):
    row_count = mix_tokens.shape[0]
    head_count = sink_logits.shape[0]
    head_dim = query_gain.shape[0]
    kv_heads = key_weight.shape[1] // head_dim
    normed = rms_scale(mix_tokens, mix_gain).astype(jnp.bfloat16)
    queries = jnp.dot(normed, query_weight, preferred_element_type=jnp.float32)
    queries = rms_scale(queries.reshape(row_count, head_count, head_dim), query_gain).astype(
        jnp.bfloat16
    )
    key_rows = jnp.dot(normed, key_weight, preferred_element_type=jnp.float32)
    key_rows = rms_scale(key_rows.reshape(row_count, kv_heads, head_dim), key_gain).astype(
        jnp.bfloat16
    )
    values = jnp.dot(normed, value_weight, preferred_element_type=jnp.float32).astype(jnp.bfloat16)
    values = values.reshape(row_count, kv_heads, head_dim)
    rim_keys, rim_values = passed_along(
        (key_rows[row_count - WINDOW :], values[row_count - WINDOW :]), ("ep", "tp"), 1
    )
    key_ext = jnp.concatenate([rim_keys, key_rows], axis=0)
    value_ext = jnp.concatenate([rim_values, values], axis=0)
    first_pos = lax.axis_index(("ep", "tp")) * row_count
    attended = window_attention(queries, key_ext, value_ext, sink_logits, first_pos)
    mix_out = jnp.dot(attended, out_weight, preferred_element_type=jnp.float32).astype(jnp.bfloat16)
    moe_rows = moe_tokens.shape[0]
    model_width = moe_tokens.shape[1]
    experts = lax.axis_size("ep")
    capacity = (9 * moe_rows * routes.shape[1] + 8 * experts - 1) // (8 * experts)
    moe_normed = rms_scale(moe_tokens, moe_gain).astype(jnp.bfloat16)
    targets = route_slots(routes, experts, capacity)
    slot_ids = jnp.arange(experts * capacity, dtype=jnp.int32)
    pick_rows = jnp.sum(
        (targets[None, :, :] == slot_ids[:, None, None]).astype(jnp.bfloat16), axis=2
    )
    packed = jnp.dot(pick_rows, moe_normed, preferred_element_type=jnp.float32).astype(jnp.bfloat16)
    reached = lax.all_to_all(
        packed.reshape(experts, 1, capacity, model_width),
        "ep",
        split_axis=0,
        concat_axis=0,
        tiled=True,
    )
    arrived_grid = lax.all_gather(reached, "tp", axis=1, tiled=True)
    gate_act = jnp.einsum(
        "etcd,df->tecf", arrived_grid, gate_weight[0], preferred_element_type=jnp.float32
    )
    up_act = jnp.einsum(
        "etcd,df->tecf", arrived_grid, up_weight[0], preferred_element_type=jnp.float32
    )
    hidden = (jax.nn.silu(gate_act) * up_act).astype(jnp.bfloat16)
    own_rows = lax.psum_scatter(
        jnp.einsum(
            "tecf,fd->tecd", hidden, down_weight[0], preferred_element_type=jnp.float32
        ).astype(jnp.bfloat16),
        "tp",
        scatter_dimension=0,
        tiled=True,
    ).astype(jnp.float32)
    returned = lax.all_to_all(
        own_rows[0].astype(jnp.bfloat16), "ep", split_axis=0, concat_axis=0, tiled=True
    )
    results = returned.reshape(experts * capacity, model_width)
    gate_probs = jax.nn.softmax(route_logits, axis=-1).astype(jnp.bfloat16)
    combine = jnp.where(
        targets[:, :, None] == slot_ids[None, None, :],
        gate_probs[:, :, None],
        jnp.zeros((), jnp.bfloat16),
    )
    combine = jnp.sum(combine, axis=1)
    moe_out = jnp.dot(combine, results, preferred_element_type=jnp.float32).astype(jnp.bfloat16)
    return (mix_out, moe_out)


def solution(mesh):
    placed = (
        P(("ep", "tp"), None),
        P(),
        P(),
        P(),
        P(),
        P(),
        P(),
        P(),
        P(),
        P(("ep", "tp"), None),
        P(),
        P(("ep", "tp"), None),
        P(("ep", "tp"), None),
        P("ep", None, "tp"),
        P("ep", None, "tp"),
        P("ep", "tp", None),
    )
    return jax.shard_map(
        body,
        mesh=mesh,
        in_specs=placed,
        out_specs=(P(("ep", "tp"), None), P(("ep", "tp"), None)),
        check_vma=False,
    )
```

profile of v0, /device:TPU:8, one launch (start us, length us, event | category | flops | bytes accessed | tf_op | source)
XLA Modules:
  0.0 282.8 jit_solution(16053804923481000589)
XLA Ops:
  10.3 1.2 fusion.17
  11.5 2.6 convolution_convert_fusion.1
  14.1 1.4 reshape.199
  15.5 30.5 %all_to_all.10 = bf16[16,1,18,2048]{3,2,1,0:T(8,128)(2,1)} all-to-all(bf16[16,1,18,2048]{3,2,1,0:T(8,128)(2,1)S(1)} %bitcast.129), channel_id=1, replica_groups=mesh['ep'=16,'tp'=8] {'ep'}, dimensions={0} | all-to-all | bytes 2359296 | tf_op jit(solution)/shard_map/all_to_all | solution.py:120
  46.2 64.4 %all-gather.2.cloned.1.call-done = bf16[16,8,18,2048]{3,2,1,0:T(8,128)(2,1)} async-done(((bf16[16,1,18,2048]{3,2,1,0:T(8,128)(2,1)}), bf16[16,8,18,2048]{3,2,1,0:T(8,128)(2,1)}) %all-gather.2.cloned.1.call-update) | async-done | bytes 9437200 | tf_op jit(solution)/shard_map/all_gather | solution.py:127
  110.5 18.8 %fusion.7 = f32[16,8,18,896]{3,2,1,0:T(8,128)} fusion(bf16[16,8,18,2048]{3,2,1,0:T(8,128)(2,1)} %all-gather.2.cloned.1.call-done, bf16[1,2048,896]{2,1,0:T(8,128)(2,1)} %param.30), kind=kOutput, calls=%fused_computation.14 | convolution fusion | flops 8455716864 | bytes 21364736 | tf_op jit(solution)/shard_map/etcd,df->tecf/dot_general | solution.py:131
  129.3 18.7 %fusion = bf16[8,16,18,896]{3,2,0,1:T(8,128)(2,1)} fusion(f32[16,8,18,896]{3,2,1,0:T(8,128)} %fusion.7, bf16[16,8,18,2048]{3,2,1,0:T(8,128)(2,1)S(1)} %copy-done.6, bf16[1,2048,896]{2,1,0:T(8,128)(2,1)} %param.29), kind=kOutput, calls=%fused_computation.1 | convolution fusion | flops 8468103168 | bytes 25493504 | tf_op jit(solution)/shard_map/etcd,df->tecf/dot_general | solution.py:128
  148.0 19.0 %convolution_convert_fusion = bf16[8,16,18,2048]{3,2,1,0:T(8,128)(2,1)} fusion(bf16[8,16,18,896]{3,2,0,1:T(8,128)(2,1)} %fusion, bf16[1,896,2048]{2,1,0:T(8,128)(2,1)} %param.31), kind=kOutput, calls=%fused_computation.7 | convolution fusion | flops 8460435456 | bytes 17235968 | tf_op jit(solution)/shard_map/tecf,fd->tecd/dot_general | solution.py:136
  167.1 1.2 copy-done.2
  170.0 2.1 collective-permute-start.1
  173.5 3.0 %collective-permute-start = (bf16[128,4,64]{0,2,1:T(8,128)(2,1)}, bf16[128,4,64]{0,2,1:T(8,128)(2,1)}, u32[]{:S(2)}, u32[]{:S(2)}) collective-permute-start(bf16[128,4,64]{0,2,1:T(8,128)(2,1)} %bitcast), channel_id=1, source_target_pairs={{0,1},{1,2},{2,3},{3,4},{4,5},{5,6},{6,7},{7,8},{8,9},{9,10},{10,1... | collective-permute-start | bytes 196616 | tf_op jit(solution)/shard_map/ppermute | solution.py:13
  177.3 5.1 %fusion.57 = (f32[256,1024]{1,0:T(8,128)}, f32[256,1024]{1,0:T(8,128)}) fusion(bf16[2048,1024]{1,0:T(8,128)(2,1)} %param.18, bf16[256,2048]{1,0:T(8,128)(2,1)S(1)} %copy-done.2, f32[2048]{0:T(1024)S(1)} %copy-done.9, f32[256]{0:T(256)S(1)} %add_rsqrt_fusion.2), kind=kOutput, calls=%fused_computation.100 | convolution fusion | flops 1076101120 | bytes 7349248 | tf_op jit(solution)/shard_map/dot_general | solution.py:91
  182.5 1.6 copy.66
  184.6 1.6 copy.67
  189.1 1.3 multiply_convert_fusion
  193.1 1.9 copy-done.1
  195.0 1.0 fusion.5
  196.0 42.9 %reduce-scatter.2.cloned.1.call-done = bf16[1,16,18,2048]{3,2,1,0:T(8,128)(2,1)} async-done(((bf16[8,16,18,2048]{3,2,1,0:T(8,128)(2,1)}), bf16[1,16,18,2048]{3,2,1,0:T(8,128)(2,1)}) %reduce-scatter.2.cloned.1.call-update) | async-done | bytes 1179664 | tf_op jit(solution)/shard_map/reduce_scatter | solution.py:135
  238.9 7.2 %all-to-all-start.1 = ((bf16[16,18,2048]{2,1,0:T(8,128)(2,1)}), bf16[16,18,2048]{2,1,0:T(8,128)(2,1)S(1)}, u32[]{:S(2)}, u32[]{:S(2)}) async-start(bf16[16,18,2048]{2,1,0:T(8,128)(2,1)} %bitcast.130), calls=%async_computation.2 | async-start | bytes 3145728 | tf_op jit(solution)/shard_map/all_to_all | solution.py:143
  246.1 3.5 %fusion.16 = bf16[2,128,4,4,64]{1,4,3,2,0:T(8,128)(2,1)S(1)} fusion(f32[2,4,256,128,4]{3,2,4,1,0:T(8,128)} %copy-done.1, f32[2,4,4,128]{3,2,1,0:T(4,128)S(1)} %exponential_add_fusion, f32[2,4,4,128]{3,2,1,0:T(4,128)S(1)} %broadcast_maximum_fusion, pred[2,128,256]{1,2,0:T(8,128)(4,1)S(1)} %broadcast_and_fusion, bf16[2,128,4,64]{1,3,2,0:T(8,128)(2,1)S(1)} %copy.63, ...), kind=kOutput, calls=%fused_computation.30 | convolution fusion | flops 140247040 | bytes 5079040 | tf_op jit(solution)/shard_map/bkgqs,bskd->bqkgd/dot_general | solution.py:62
  250.2 2.3 convolution_convert_fusion.2
  252.4 19.8 %all-to-all-done.1 = bf16[16,18,2048]{2,1,0:T(8,128)(2,1)S(1)} async-done(((bf16[16,18,2048]{2,1,0:T(8,128)(2,1)}), bf16[16,18,2048]{2,1,0:T(8,128)(2,1)S(1)}, u32[]{:S(2)}, u32[]{:S(2)}) %all-to-all-start.1) | async-done | bytes 1179680 | tf_op jit(solution)/shard_map/all_to_all | solution.py:143
  272.2 1.2 reshape.200
  273.4 2.5 convolution_convert_fusion.3
  (70 shorter events, 13.7 us)
Async XLA Ops:
  7.2 161.4 %copy-start = (bf16[2048,256]{1,0:T(8,128)(2,1)S(1)}, bf16[2048,256]{1,0:T(8,128)(2,1)}, u32[]{:S(2)}) copy-start(bf16[2048,256]{1,0:T(8,128)(2,1)} %param.19) | copy-start | bytes 3145732
  7.2 103.3 %all-gather.2.cloned.1.call-start = ((), (), s32[]{:S(2)}) async-start(), calls=%async_computation.3 | async-start | bytes 14155776 | tf_op jit(solution)/shard_map/all_gather | solution.py:127
  46.1 192.8 %reduce-scatter.2.cloned.1.call-start = ((), (), s32[]{:S(2)}) async-start(), calls=%async_computation.4 | async-start | bytes 14155776 | tf_op jit(solution)/shard_map/reduce_scatter | solution.py:135
  110.5 18.8 %copy-start.6 = (bf16[16,8,18,2048]{3,2,1,0:T(8,128)(2,1)S(1)}, bf16[16,8,18,2048]{3,2,1,0:T(8,128)(2,1)}, u32[]{:S(2)}) copy-start(bf16[16,8,18,2048]{3,2,1,0:T(8,128)(2,1)} %all-gather.2.cloned.1.call-done) | copy-start | bytes 28311556
  167.0 1.2 copy-start.2
  167.0 1.5 copy-start.9
  167.0 2.2 copy-start.5
  168.3 3.9 %copy-start.8 = (bf16[2048,256]{1,0:T(8,128)(2,1)S(1)}, bf16[2048,256]{1,0:T(8,128)(2,1)}, u32[]{:S(2)}) copy-start(bf16[2048,256]{1,0:T(8,128)(2,1)} %param.20) | copy-start | bytes 3145732
  170.0 20.4 %collective-permute-start.1 = (bf16[128,4,64]{0,2,1:T(8,128)(2,1)}, bf16[128,4,64]{0,2,1:T(8,128)(2,1)}, u32[]{:S(2)}, u32[]{:S(2)}) collective-permute-start(bf16[128,4,64]{0,2,1:T(8,128)(2,1)} %slice.29), channel_id=1, source_target_pairs={{0,1},{1,2},{2,3},{3,4},{4,5},{5,6},{6,7},{7,8},{8,9},{9,10},{10,1... | collective-permute-start | bytes 196616 | tf_op jit(solution)/shard_map/ppermute | solution.py:13
  172.8 9.6 %copy-start.3 = (bf16[256,256]{0,1:T(8,128)(2,1)}, bf16[256,256]{0,1:T(8,128)(2,1)S(1)}, u32[]{:S(2)}) copy-start(bf16[256,256]{0,1:T(8,128)(2,1)S(1)} %convolution_convert_fusion.4) | copy-start | bytes 393220
  173.5 17.8 %collective-permute-start = (bf16[128,4,64]{0,2,1:T(8,128)(2,1)}, bf16[128,4,64]{0,2,1:T(8,128)(2,1)}, u32[]{:S(2)}, u32[]{:S(2)}) collective-permute-start(bf16[128,4,64]{0,2,1:T(8,128)(2,1)} %bitcast), channel_id=1, source_target_pairs={{0,1},{1,2},{2,3},{3,4},{4,5},{5,6},{6,7},{7,8},{8,9},{9,10},{10,1... | collective-permute-start | bytes 196616 | tf_op jit(solution)/shard_map/ppermute | solution.py:13
  182.5 5.5 %copy-start.4 = (f32[128,2]{0,1:T(2,128)S(1)}, f32[128,2]{0,1:T(2,128)}, u32[]{:S(2)}) copy-start(f32[128,2]{0,1:T(2,128)} %param.28) | copy-start | bytes 3076
  193.0 2.0 copy-start.1
  238.9 33.3 %all-to-all-start.1 = ((bf16[16,18,2048]{2,1,0:T(8,128)(2,1)}), bf16[16,18,2048]{2,1,0:T(8,128)(2,1)S(1)}, u32[]{:S(2)}, u32[]{:S(2)}) async-start(bf16[16,18,2048]{2,1,0:T(8,128)(2,1)} %bitcast.130), calls=%async_computation.2 | async-start | bytes 3145728 | tf_op jit(solution)/shard_map/all_to_all | solution.py:143
  246.1 4.1 %copy-start.7 = (bf16[1024,2048]{1,0:T(8,128)(2,1)S(1)}, bf16[1024,2048]{1,0:T(8,128)(2,1)}, u32[]{:S(2)}) copy-start(bf16[1024,2048]{1,0:T(8,128)(2,1)} %param.24) | copy-start | bytes 12582916
Sparse Core Ops, SparseCore 0:
  46.2 64.2 all-gather.1
  167.2 71.6 reduce-scatter.1
where the time goes:
time: 283 us
  waiting for transfers between devices  127 us (45%)
  matrix products  74.7 us (26%)
  blocking collectives  30.5 us (11%)
  local copies, waits for them, and re-layouts  15.3 us (5%)
  between operations  14.4 us (5%)
  starting transfers between devices  12.3 us (4%)
  other arithmetic  8.43 us (3%)
    all_gather x1, waiting for transfers between devices, body(): arrived_grid = lax.all_gather(reached, 'tp', axis=1, tiled=True)  64.4 us
    reduce_scatter x1, waiting for transfers between devices, body(): lax.psum_scatter(jnp.einsum('tecf,fd->tecd', hidden, down_weight[0], pref...  42.9 us
    all_to_all x1, blocking collectives, body(): lax.all_to_all(packed.reshape(experts, 1, capacity, model_width), 'ep', s...  30.5 us
    all_to_all x1, waiting for transfers between devices, body(): lax.all_to_all(own_rows[0].astype(jnp.bfloat16), 'ep', split_axis=0, conc...  19.8 us
    dot_general x1, matrix products, body(): jnp.einsum('tecf,fd->tecd', hidden, down_weight[0], preferred_element_typ...  19 us
    dot_general x1, matrix products, body(): jnp.einsum('etcd,df->tecf', arrived_grid, up_weight[0], preferred_element...  18.8 us
    dot_general x1, matrix products, body(): jnp.einsum('etcd,df->tecf', arrived_grid, gate_weight[0], preferred_eleme...  18.7 us
    all_to_all x1, starting transfers between devices, body(): lax.all_to_all(own_rows[0].astype(jnp.bfloat16), 'ep', split_axis=0, conc...  7.15 us
  transfers between devices with their start and end apart: 5, of which 3 were waited for; matrix products, arithmetic and copies ran while one was open for 9% of the time, Pallas kernels for 0%

commit v1 on v0

--- a/solution.py
+++ b/solution.py
@@ -124,7 +124,9 @@
         concat_axis=0,
         tiled=True,
     )
-    arrived_grid = lax.all_gather(reached, "tp", axis=1, tiled=True)
+    arrived_grid = jnp.concatenate(
+        lax.all_to_all(jnp.stack([reached] * lax.axis_size("tp")), "tp", 0, 0), axis=1
+    )
     gate_act = jnp.einsum(
         "etcd,df->tecf", arrived_grid, gate_weight[0], preferred_element_type=jnp.float32
     )

time: 283 us -> 355 us (1.25); the launches traced: 283 us -> 351 us
  blocking collectives: 30.5 us -> 142 us
  waiting for transfers between devices: 127 us -> 59.9 us
  matrix products: 74.7 us -> 94.7 us
  local copies, waits for them, and re-layouts: 15.3 us -> 20.8 us
    all_to_all x0 -> x1, blocking collectives: none -> 111 us  [body(): lax.all_to_all(jnp.stack([reached] * lax.axis_size('tp')), 'tp', 0, 0)]
    all_gather x1 -> x0, waiting for transfers between devices: 64.4 us -> none  [body(): arrived_grid = lax.all_gather(reached, 'tp', axis=1, tiled=True)]
    dot_general x1, matrix products: 18.7 us -> 30.8 us  [body(): jnp.einsum('etcd,df->tecf', arrived_grid, gate_weight[0], preferred_eleme...]
    dot_general x1, matrix products: 18.8 us -> 27.6 us  [body(): jnp.einsum('etcd,df->tecf', arrived_grid, up_weight[0], preferred_element...]
    unnamed x21 -> x27, local copies, waits for them, and re-layouts: 3.97 us -> 7.56 us
  transfers between devices with their start and end apart: 5 -> 4, of which waited for: 3 -> 2; matrix products, arithmetic and copies ran while one was open for 9% -> 8% of each run, Pallas kernels for 0% -> 0%
where the time goes in v1:
time: 355 us; the launch traced here: 351 us
  blocking collectives  142 us (40%)
  matrix products  94.7 us (27%)
  waiting for transfers between devices  59.9 us (17%)
  local copies, waits for them, and re-layouts  20.8 us (6%)
  between operations  14.6 us (4%)
  starting transfers between devices  10.6 us (3%)
  other arithmetic  8.44 us (2%)
    all_to_all x1, blocking collectives, body(): lax.all_to_all(jnp.stack([reached] * lax.axis_size('tp')), 'tp', 0, 0)  111 us
    reduce_scatter x1, waiting for transfers between devices, body(): lax.psum_scatter(jnp.einsum('tecf,fd->tecd', hidden, down_weight[0], pref...  40.1 us
    dot_general x1, matrix products, body(): jnp.einsum('etcd,df->tecf', arrived_grid, gate_weight[0], preferred_eleme...  30.8 us
    all_to_all x1, blocking collectives, body(): lax.all_to_all(packed.reshape(experts, 1, capacity, model_width), 'ep', s...  30.4 us
    dot_general x1, matrix products, body(): jnp.einsum('etcd,df->tecf', arrived_grid, up_weight[0], preferred_element...  27.6 us
    all_to_all x1, waiting for transfers between devices, body(): lax.all_to_all(own_rows[0].astype(jnp.bfloat16), 'ep', split_axis=0, conc...  19.8 us
    dot_general x1, matrix products, body(): jnp.einsum('tecf,fd->tecd', hidden, down_weight[0], preferred_element_typ...  18.4 us
    unnamed x27, local copies, waits for them, and re-layouts  7.56 us
  transfers between devices with their start and end apart: 4, of which 2 were waited for; matrix products, arithmetic and copies ran while one was open for 8% of the time, Pallas kernels for 0%

profile of v1, /device:TPU:8, one launch (start us, length us, event | category | flops | bytes accessed | tf_op | source)
XLA Modules:
  0.0 350.8 jit_solution(5487714742276406490)
XLA Ops:
  10.3 1.2 fusion.24
  11.5 2.6 convolution_convert_fusion.1
  14.1 1.4 reshape.208
  15.5 30.4 %all_to_all.18 = bf16[16,1,18,2048]{3,2,1,0:T(8,128)(2,1)S(1)} all-to-all(bf16[16,1,18,2048]{3,2,1,0:T(8,128)(2,1)S(1)} %bitcast.137), channel_id=1, replica_groups=mesh['ep'=16,'tp'=8] {'ep'}, dimensions={0} | all-to-all | bytes 2359296 | tf_op jit(solution)/shard_map/all_to_all | solution.py:120
  46.6 1.2 stack.2
  47.9 111.4 %all_to_all.19 = bf16[8,16,1,18,2048]{4,1,3,2,0:T(8,128)(2,1)S(1)} all-to-all(bf16[8,16,1,18,2048]{4,1,3,2,0:T(8,128)(2,1)S(1)} %stack.2), channel_id=1, replica_groups=mesh['ep'=16,'tp'=8] {'tp'}, dimensions={0} | all-to-all | bytes 18874368 | tf_op jit(solution)/shard_map/all_to_all | solution.py:128
  159.2 3.6 %copy-done.1 = bf16[8,16,1,18,2048]{4,1,3,2,0:T(8,128)(2,1)} copy-done((bf16[8,16,1,18,2048]{4,1,3,2,0:T(8,128)(2,1)}, bf16[8,16,1,18,2048]{4,1,3,2,0:T(8,128)(2,1)S(1)}, u32[]{:S(2)}) %copy-start.1) | copy-done | bytes 9437208
  162.8 27.6 %fusion = f32[16,8,18,896]{3,2,1,0:T(8,128)} fusion(bf16[8,16,1,18,2048]{4,1,3,2,0:T(8,128)(2,1)S(1)} %all_to_all.19, bf16[1,2048,896]{2,1,0:T(8,128)(2,1)S(1)} %copy-done.8), kind=kOutput, calls=%fused_computation | convolution fusion | flops 8455716864 | bytes 21364736 | tf_op jit(solution)/shard_map/etcd,df->tecf/dot_general | solution.py:133
  190.4 30.8 %fusion.6 = bf16[8,16,18,896]{3,2,0,1:T(8,128)(2,1)} fusion(f32[16,8,18,896]{3,2,1,0:T(8,128)} %fusion, bf16[8,16,1,18,2048]{4,1,3,2,0:T(8,128)(2,1)} %copy-done.1, bf16[1,2048,896]{2,1,0:T(8,128)(2,1)S(1)} %copy-done.9), kind=kOutput, calls=%fused_computation.7 | convolution fusion | flops 8468103168 | bytes 25493504 | tf_op jit(solution)/shard_map/etcd,df->tecf/dot_general | solution.py:130
  221.2 18.4 %convolution_convert_fusion = bf16[8,16,18,2048]{3,2,1,0:T(8,128)(2,1)} fusion(bf16[8,16,18,896]{3,2,0,1:T(8,128)(2,1)} %fusion.6, bf16[1,896,2048]{2,1,0:T(8,128)(2,1)S(1)} %copy-done.10), kind=kOutput, calls=%fused_computation.13 | convolution fusion | flops 8460435456 | bytes 17235968 | tf_op jit(solution)/shard_map/tecf,fd->tecd/dot_general | solution.py:138
  239.6 1.2 copy-done.3
  242.6 1.9 collective-permute-start.1
  245.9 1.9 collective-permute-start
  248.6 4.9 %fusion.64 = (f32[256,1024]{1,0:T(8,128)}, f32[256,1024]{1,0:T(8,128)}) fusion(bf16[2048,1024]{1,0:T(8,128)(2,1)} %param.18, bf16[256,2048]{1,0:T(8,128)(2,1)S(1)} %copy-done.3, f32[2048]{0:T(1024)S(1)} %copy-done.12, f32[256]{0:T(256)S(1)} %add_rsqrt_fusion.2), kind=kOutput, calls=%fused_computation.105 | convolution fusion | flops 1076101120 | bytes 7349248 | tf_op jit(solution)/shard_map/dot_general | solution.py:91
  253.5 1.6 copy.85
  255.6 1.6 copy.86
  260.2 1.3 multiply_convert_fusion
  264.2 1.9 copy-done.2
  267.1 40.1 %reduce-scatter.2.cloned.1.call-done = bf16[1,16,18,2048]{3,2,1,0:T(8,128)(2,1)} async-done(((bf16[8,16,18,2048]{3,2,1,0:T(8,128)(2,1)}), bf16[1,16,18,2048]{3,2,1,0:T(8,128)(2,1)}) %reduce-scatter.2.cloned.1.call-update) | async-done | bytes 1179664 | tf_op jit(solution)/shard_map/reduce_scatter | solution.py:137
  307.1 6.7 %all-to-all-start.2 = ((bf16[16,18,2048]{2,1,0:T(8,128)(2,1)}), bf16[16,18,2048]{2,1,0:T(8,128)(2,1)S(1)}, u32[]{:S(2)}, u32[]{:S(2)}) async-start(bf16[16,18,2048]{2,1,0:T(8,128)(2,1)} %bitcast.139), calls=%async_computation.3 | async-start | bytes 3145728 | tf_op jit(solution)/shard_map/all_to_all | solution.py:145
  313.9 3.5 %fusion.23 = bf16[2,128,4,4,64]{1,4,3,2,0:T(8,128)(2,1)S(1)} fusion(f32[2,4,256,128,4]{3,2,4,1,0:T(8,128)} %copy-done.2, f32[2,4,4,128]{3,2,1,0:T(4,128)S(1)} %exponential_add_fusion, f32[2,4,4,128]{3,2,1,0:T(4,128)S(1)} %broadcast_maximum_fusion, pred[2,128,256]{1,2,0:T(8,128)(4,1)S(1)} %broadcast_and_fusion, bf16[2,128,4,64]{1,3,2,0:T(8,128)(2,1)S(1)} %copy.82, ...), kind=kOutput, calls=%fused_computation.35 | convolution fusion | flops 140247040 | bytes 5079040 | tf_op jit(solution)/shard_map/bkgqs,bskd->bqkgd/dot_general | solution.py:62
  318.0 2.3 convolution_convert_fusion.2
  320.2 19.8 %all-to-all-done.2 = bf16[16,18,2048]{2,1,0:T(8,128)(2,1)S(1)} async-done(((bf16[16,18,2048]{2,1,0:T(8,128)(2,1)}), bf16[16,18,2048]{2,1,0:T(8,128)(2,1)S(1)}, u32[]{:S(2)}, u32[]{:S(2)}) %all-to-all-start.2) | async-done | bytes 1179680 | tf_op jit(solution)/shard_map/all_to_all | solution.py:145
  341.2 2.5 convolution_convert_fusion.3
  (76 shorter events, 16.4 us)
Async XLA Ops:
  7.2 234.0 %copy-start = (bf16[2048,256]{1,0:T(8,128)(2,1)S(1)}, bf16[2048,256]{1,0:T(8,128)(2,1)}, u32[]{:S(2)}) copy-start(bf16[2048,256]{1,0:T(8,128)(2,1)} %param.19) | copy-start | bytes 3145732
  7.2 300.0 %reduce-scatter.2.cloned.1.call-start = ((), (), s32[]{:S(2)}) async-start(), calls=%async_computation.4 | async-start | bytes 14155776 | tf_op jit(solution)/shard_map/reduce_scatter | solution.py:137
  47.9 114.9 %copy-start.8 = (bf16[1,2048,896]{2,1,0:T(8,128)(2,1)S(1)}, bf16[1,2048,896]{2,1,0:T(8,128)(2,1)}, u32[]{:S(2)}) copy-start(bf16[1,2048,896]{2,1,0:T(8,128)(2,1)} %param.30) | copy-start | bytes 11010052
  159.2 3.6 %copy-start.1 = (bf16[8,16,1,18,2048]{4,1,3,2,0:T(8,128)(2,1)}, bf16[8,16,1,18,2048]{4,1,3,2,0:T(8,128)(2,1)S(1)}, u32[]{:S(2)}) copy-start(bf16[8,16,1,18,2048]{4,1,3,2,0:T(8,128)(2,1)S(1)} %all_to_all.19) | copy-start | bytes 28311556
  162.8 27.6 %copy-start.9 = (bf16[1,2048,896]{2,1,0:T(8,128)(2,1)S(1)}, bf16[1,2048,896]{2,1,0:T(8,128)(2,1)}, u32[]{:S(2)}) copy-start(bf16[1,2048,896]{2,1,0:T(8,128)(2,1)} %param.29) | copy-start | bytes 11010052
  190.4 30.8 %copy-start.10 = (bf16[1,896,2048]{2,1,0:T(8,128)(2,1)S(1)}, bf16[1,896,2048]{2,1,0:T(8,128)(2,1)}, u32[]{:S(2)}) copy-start(bf16[1,896,2048]{2,1,0:T(8,128)(2,1)} %param.31) | copy-start | bytes 11010052
  239.6 1.2 copy-start.3
  239.6 1.5 copy-start.12
  239.6 2.2 copy-start.6
  240.8 3.7 %copy-start.11 = (bf16[2048,256]{1,0:T(8,128)(2,1)S(1)}, bf16[2048,256]{1,0:T(8,128)(2,1)}, u32[]{:S(2)}) copy-start(bf16[2048,256]{1,0:T(8,128)(2,1)} %param.20) | copy-start | bytes 3145732
  242.6 19.0 %collective-permute-start.1 = (bf16[128,4,64]{0,2,1:T(8,128)(2,1)}, bf16[128,4,64]{0,2,1:T(8,128)(2,1)}, u32[]{:S(2)}, u32[]{:S(2)}) collective-permute-start(bf16[128,4,64]{0,2,1:T(8,128)(2,1)} %slice.29), channel_id=1, source_target_pairs={{0,1},{1,2},{2,3},{3,4},{4,5},{5,6},{6,7},{7,8},{8,9},{9,10},{10,1... | collective-permute-start | bytes 196616 | tf_op jit(solution)/shard_map/ppermute | solution.py:13
  245.2 8.3 %copy-start.4 = (bf16[256,256]{0,1:T(8,128)(2,1)}, bf16[256,256]{0,1:T(8,128)(2,1)S(1)}, u32[]{:S(2)}) copy-start(bf16[256,256]{0,1:T(8,128)(2,1)S(1)} %convolution_convert_fusion.4) | copy-start | bytes 393220
  245.9 16.5 %collective-permute-start = (bf16[128,4,64]{0,2,1:T(8,128)(2,1)}, bf16[128,4,64]{0,2,1:T(8,128)(2,1)}, u32[]{:S(2)}, u32[]{:S(2)}) collective-permute-start(bf16[128,4,64]{0,2,1:T(8,128)(2,1)} %bitcast), channel_id=1, source_target_pairs={{0,1},{1,2},{2,3},{3,4},{4,5},{5,6},{6,7},{7,8},{8,9},{9,10},{10,1... | collective-permute-start | bytes 196616 | tf_op jit(solution)/shard_map/ppermute | solution.py:13
  253.5 5.6 %copy-start.5 = (f32[128,2]{0,1:T(2,128)S(1)}, f32[128,2]{0,1:T(2,128)}, u32[]{:S(2)}) copy-start(f32[128,2]{0,1:T(2,128)} %param.28) | copy-start | bytes 3076
  264.1 2.0 copy-start.2
  307.1 32.9 %all-to-all-start.2 = ((bf16[16,18,2048]{2,1,0:T(8,128)(2,1)}), bf16[16,18,2048]{2,1,0:T(8,128)(2,1)S(1)}, u32[]{:S(2)}, u32[]{:S(2)}) async-start(bf16[16,18,2048]{2,1,0:T(8,128)(2,1)} %bitcast.139), calls=%async_computation.3 | async-start | bytes 3145728 | tf_op jit(solution)/shard_map/all_to_all | solution.py:145
  313.9 4.1 %copy-start.7 = (bf16[1024,2048]{1,0:T(8,128)(2,1)S(1)}, bf16[1024,2048]{1,0:T(8,128)(2,1)}, u32[]{:S(2)}) copy-start(bf16[1024,2048]{1,0:T(8,128)(2,1)} %param.24) | copy-start | bytes 12582916
Sparse Core Ops, SparseCore 0:
  239.8 67.3 reduce-scatter.1
